TPU v7x, 32 devices: a whole 2x2x4 slice. The times are simulated.
32 devices in a mesh: fs: 8 (over z, y), tp: 4 (over x, core).
Axes of the slice: x: 2, y: 2, z: 4, core: 2. Of those that a mesh axis runs over, the one named last changes fastest.
Arguments:
- inputs: bfloat16 [6144, 2048], P('fs'), may hold values from -6 to 6
- values_cot: bfloat16 [6144, 2048], P('fs', 'tp'), may hold values from -0.22949219 to 0.22949219
- decay_cot: bfloat16 [6144, 16], P('fs'), may hold values from -0.22949219 to 0.22949219
- factor: bfloat16 [2048, 512], P('fs', 'tp'), may hold values from -0.125 to 0.125
- value_weight: float32 [2048, 2048], P('fs', 'tp'), may hold values from -3 to 3
- lowrank_mean: float32 [512, 2048], P('fs', 'tp'), may hold values from -60 to 60
- lowrank_var: float32 [512, 2048], P('fs', 'tp'), may hold values from 0.3 to 3
- decay_weight: float32 [2048, 16], replicated, may hold values from -3 to 3
- decay_mean: float32 [2048, 16], replicated, may hold values from -6 to 6
- decay_var: float32 [2048, 16], replicated, may hold values from 0.3 to 3
Outputs:
- value_step: float32 [2048, 2048], P('fs', 'tp')
- value_new: float32 [2048, 2048], P('fs', 'tp')
- value_copy: bfloat16 [2048, 2048], P('fs', 'tp')
- mean_new: float32 [512, 2048], P('fs', 'tp')
- var_new: float32 [512, 2048], P('fs', 'tp')
- decay_new: float32 [2048, 16], replicated
- decay_copy: bfloat16 [2048, 16], replicated
- decay_mean_new: float32 [2048, 16], replicated
- decay_var_new: float32 [2048, 16], replicated
All inputs are finite; a program needn't handle non-finite values.
Results may differ from a plain program's by a relative error of at most 0.0042.
Values may be sent and summed in bfloat16 or wider, within the bound.
A program may use at most 64 MiB of HBM per device.

v0:
```python
import jax
import jax.numpy as jnp
from jax import lax
from jax.sharding import PartitionSpec as P

W = 2048
R = 512


def local(
    inputs,
    values_cot,
    decay_cot,
    factor,
    value_weight,
    lowrank_mean,
    lowrank_var,
    decay_weight,
    decay_mean,
    decay_var,
):
    own_rows = lax.all_gather(factor, "tp", axis=1, tiled=True)
    quarter = jnp.dot(
        inputs, lax.all_gather(factor, "fs", axis=0, tiled=True), preferred_element_type=jnp.float32
    ).astype(jnp.bfloat16)
    projected = lax.all_gather(quarter, "tp", axis=1, tiled=True)
    lowrank_grad = lax.psum_scatter(
        lax.dot_general(
            projected, values_cot, (((0,), (0,)), ((), ())), preferred_element_type=jnp.float32
        ),
        "fs",
        scatter_dimension=0,
        tiled=True,
    )
    mean_new = 0.9 * lowrank_mean + 0.1 * lowrank_grad
    var_new = 0.95 * lowrank_var + 0.05 * lowrank_grad * lowrank_grad
    adam_ratio = mean_new / (jnp.sqrt(var_new) + 1e-08)
    full_ratio = lax.all_gather(adam_ratio, "fs", axis=0, tiled=True)
    squares = lax.psum(jnp.sum(adam_ratio * adam_ratio), ("fs", "tp"))
    root_mean = jnp.sqrt(squares / (R * W) + 1e-06)
    delta = jnp.dot(own_rows.astype(jnp.float32), full_ratio, precision=lax.Precision.HIGHEST)
    value_step = -0.5 / root_mean * delta
    value_new = value_weight + value_step
    value_copy = value_new.astype(jnp.bfloat16)
    decay_part = lax.dot_general(
        inputs, decay_cot, (((0,), (0,)), ((), ())), preferred_element_type=jnp.float32
    )
    decay_grad = lax.psum(decay_part, "fs")
    decay_mean_new = 0.9 * decay_mean + 0.1 * decay_grad
    decay_var_new = 0.95 * decay_var + 0.05 * decay_grad * decay_grad
    decay_new = decay_weight - 0.5 * decay_mean_new / (jnp.sqrt(decay_var_new) + 1e-08)
    decay_copy = decay_new.astype(jnp.bfloat16)
    return (
        value_step,
        value_new,
        value_copy,
        mean_new,
        var_new,
        decay_new,
        decay_copy,
        decay_mean_new,
        decay_var_new,
    )


def solution(mesh):
    in_specs = (
        P("fs", None),
        P("fs", "tp"),
        P("fs", None),
        P("fs", "tp"),
        P("fs", "tp"),
        P("fs", "tp"),
        P("fs", "tp"),
        P(),
        P(),
        P(),
    )
    out_specs = (
        P("fs", "tp"),
        P("fs", "tp"),
        P("fs", "tp"),
        P("fs", "tp"),
        P("fs", "tp"),
        P(),
        P(),
        P(),
        P(),
    )
    return jax.shard_map(local, mesh=mesh, in_specs=in_specs, out_specs=out_specs, check_vma=False)
```

profile of v0, /device:TPU:0, one launch (start us, length us, event | category | flops | bytes accessed | tf_op | source)
XLA Modules:
  0.0 248.1 jit_solution(9775094986767670953)
XLA Ops:
  7.2 0.0 copy-start
  7.2 0.0 reduce-scatter.2.cloned.1.call-start
  7.2 33.4 %all_gather.12 = bf16[2048,128]{1,0:T(8,128)(2,1)S(1)} all-gather(bf16[256,128]{1,0:T(8,128)(2,1)} %param.13), channel_id=1, replica_groups=mesh['fs'=8,'tp'=4] {'fs'}, dimensions={0}, use_global_device_ids=true | all-gather | bytes 589824 | tf_op jit(solution)/shard_map/all_gather | solution.py:24
  40.6 0.0 copy-done
  40.6 0.0 copy-start.1
  40.6 1.0 convolution_convert_fusion
  41.6 0.0 copy-start.5
  41.6 8.6 %all_gather.13 = bf16[768,512]{1,0:T(8,128)(2,1)S(1)} all-gather(bf16[768,128]{1,0:T(8,128)(2,1)S(1)} %convolution_convert_fusion), channel_id=1, replica_groups=mesh['fs'=8,'tp'=4] {'tp'}, dimensions={1}, use_global_device_ids=true | all-gather | bytes 983040 | tf_op jit(solution)/shard_map/all_gather | solution.py:26
  50.2 0.0 copy-done.1
  50.2 1.6 fusion.7
  51.8 0.0 reduce-scatter.2.cloned.1.call-update
  51.8 0.0 all-reduce.2.cloned.1.call-start
  51.9 0.0 copy-done.5
  51.9 1.2 fusion.8
  53.1 0.0 all-reduce.2.cloned.1.call-update
  53.1 0.0 all-gather.2.cloned.1.call-start
  53.2 63.2 %reduce-scatter.2.cloned.1.call-done = f32[64,512]{1,0:T(8,128)} async-done(((f32[512,512]{1,0:T(8,128)}), f32[64,512]{1,0:T(8,128)}) %reduce-scatter.2.cloned.1.call-update) | async-done | bytes 131088 | tf_op jit(solution)/shard_map/reduce_scatter | solution.py:27
  116.3 0.0 copy-done.3
  116.3 0.0 copy-done.4
  116.3 2.3 multiply_reduce_fusion
  118.6 0.0 all-gather.2.cloned.1.call-update
  118.6 2.0 copy.19
  120.7 0.0 copy-done.2
  120.7 5.8 %all_gather.15 = bf16[256,512]{1,0:T(8,128)(2,1)S(1)} all-gather(bf16[256,128]{1,0:T(8,128)(2,1)S(1)} %copy-done.2), channel_id=1, replica_groups=mesh['fs'=8,'tp'=4] {'tp'}, dimensions={1}, use_global_device_ids=true | all-gather | bytes 327680 | tf_op jit(solution)/shard_map/all_gather | solution.py:22
  126.5 63.3 %all-reduce.2.cloned.1.call-done = f32[2048,16]{0,1:T(8,128)} async-done(((f32[2048,16]{0,1:T(8,128)}), f32[2048,16]{0,1:T(8,128)}) %all-reduce.2.cloned.1.call-update) | async-done | bytes 131088 | tf_op jit(solution)/shard_map/psum | solution.py:48
  189.7 1.9 fusion.3
  191.6 39.9 %psum.14 = f32[]{:T(128)} all-reduce(f32[]{:T(128)} %get-tuple-element.24), channel_id=1, replica_groups=mesh['fs'=8,'tp'=4] {'fs','tp'}, use_global_device_ids=true, to_apply=%region_2.0 | all-reduce | flops 1 | bytes 8 | tf_op jit(solution)/shard_map/psum | solution.py:39
  232.3 0.0 all-gather.2.cloned.1.call-done
  232.3 3.4 %fusion.5 = (bf16[256,512]{0,1:T(8,128)(2,1)}, f32[256,512]{0,1:T(8,128)}, f32[256,512]{0,1:T(8,128)}) fusion(f32[256,512]{0,1:T(8,128)} %copy.19, f32[512,512]{1,0:T(8,128)} %all-gather.2.cloned.1.call-done, bf16[256,512]{1,0:T(8,128)(2,1)S(1)} %all_gather.15, f32[]{:T(128)S(6)} %div.14), kind=kOutput, calls=%fused_computation.13 | convolution fusion | flops 805699584 | bytes 3145732 | tf_op jit(solution)/shard_map/dot_general | solution.py:41
  235.7 2.0 copy.20
  237.7 2.0 copy.21
  239.8 1.8 copy.22
  (3 shorter events, 0.0 us)
Async XLA Ops:
  7.2 33.4 %copy-start = (bf16[768,2048]{1,0:T(8,128)(2,1)S(1)}, bf16[768,2048]{1,0:T(8,128)(2,1)}, u32[]{:S(2)}) copy-start(bf16[768,2048]{1,0:T(8,128)(2,1)} %param.10) | copy-start | bytes 9437188
  7.2 109.1 %reduce-scatter.2.cloned.1.call-start = ((), (), s32[]{:S(2)}) async-start(), calls=%async_computation.1 | async-start | bytes 1179648 | tf_op jit(solution)/shard_map/reduce_scatter | solution.py:27
  40.6 9.6 %copy-start.1 = (bf16[768,512]{1,0:T(8,128)(2,1)S(1)}, bf16[768,512]{1,0:T(8,128)(2,1)}, u32[]{:S(2)}) copy-start(bf16[768,512]{1,0:T(8,128)(2,1)} %param.11) | copy-start | bytes 2359300
  41.6 10.3 %copy-start.5 = (bf16[768,16]{0,1:T(8,128)(2,1)S(1)}, bf16[768,16]{0,1:T(8,128)(2,1)}, u32[]{:S(2)}) copy-start(bf16[768,16]{0,1:T(8,128)(2,1)} %param.12) | copy-start | bytes 73732
  50.2 66.1 %copy-start.3 = (f32[64,512]{1,0:T(8,128)S(1)}, f32[64,512]{1,0:T(8,128)}, u32[]{:S(2)}) copy-start(f32[64,512]{1,0:T(8,128)} %param.16) | copy-start | bytes 393220
  50.2 66.1 %copy-start.4 = (f32[64,512]{1,0:T(8,128)S(1)}, f32[64,512]{1,0:T(8,128)}, u32[]{:S(2)}) copy-start(f32[64,512]{1,0:T(8,128)} %param.15) | copy-start | bytes 393220
  51.8 68.9 %copy-start.2 = (bf16[256,128]{1,0:T(8,128)(2,1)S(1)}, bf16[256,128]{1,0:T(8,128)(2,1)}, u32[]{:S(2)}) copy-start(bf16[256,128]{1,0:T(8,128)(2,1)} %param.13) | copy-start | bytes 196612
  51.8 137.9 %all-reduce.2.cloned.1.call-start = ((), (), s32[]{:S(2)}) async-start(), calls=%async_computation.3 | async-start | bytes 262144 | tf_op jit(solution)/shard_map/psum | solution.py:48
  53.1 179.2 %all-gather.2.cloned.1.call-start = ((), (), s32[]{:S(2)}) async-start(), calls=%async_computation.2 | async-start | bytes 1179648 | tf_op jit(solution)/shard_map/all_gather | solution.py:38
Sparse Core Ops, SparseCore 0:
  52.0 64.3 reduce-scatter.1
  120.3 69.4 all-reduce.1
  192.4 39.6 all-gather.1
where the time goes:
time: 249 us; the launch traced here: 248 us
  waiting for transfers between devices  127 us (51%)
  blocking collectives  87.7 us (35%)
  between operations  14.5 us (6%)
  local copies, waits for them, and re-layouts  7.93 us (3%)
  matrix products  7.14 us (3%)
  other arithmetic  4.16 us (2%)
    psum x1, waiting for transfers between devices, local(): decay_grad = lax.psum(decay_part, 'fs')  63.3 us
    reduce_scatter x1, waiting for transfers between devices, local(): lax.psum_scatter(lax.dot_general(projected, values_cot, (((0,), (0,)), ((...  63.2 us
    psum x1, blocking collectives, local(): squares = lax.psum(jnp.sum(adam_ratio * adam_ratio), ('fs', 'tp'))  39.9 us
    all_gather x1, blocking collectives, local(): lax.all_gather(factor, 'fs', axis=0, tiled=True)  33.4 us
    all_gather x1, blocking collectives, local(): projected = lax.all_gather(quarter, 'tp', axis=1, tiled=True)  8.62 us
    unnamed x16, local copies, waits for them, and re-layouts  7.93 us
    all_gather x1, blocking collectives, local(): own_rows = lax.all_gather(factor, 'tp', axis=1, tiled=True)  5.79 us
  transfers between devices with their start and end apart: 3, of which 2 were waited for; matrix products, arithmetic and copies ran while one was open for 3% of the time, Pallas kernels for 0%

commit v1 on v0

v1 whole, which is shorter than its diff:
```python
import functools

import jax
import jax.numpy as jnp
from jax import lax
from jax.experimental import pallas as pl
from jax.experimental.pallas import tpu as pltpu
from jax.sharding import PartitionSpec as P

MESH = pl.DeviceIdType.MESH
F32 = jnp.float32
BF16 = jnp.bfloat16


def moments(mean, var, grad):
    return 0.9 * mean + 0.1 * grad, 0.95 * var + 0.05 * grad * grad


def remote(src, dst, send_sem, recv_sem, axis, peer):
    return pltpu.make_async_remote_copy(
        src_ref=src,
        dst_ref=dst,
        send_sem=send_sem,
        recv_sem=recv_sem,
        device_id={axis: peer},
        device_id_type=MESH,
    )


class Gather:
    def __init__(self, axis, size, view, send_sems, recv_sems, pending):
        self.axis, self.view, self.pending = axis, view, pending
        self.send_sems, self.recv_sems = send_sems, recv_sems
        self.me = lax.axis_index(axis)
        self.groups = size // 2
        self.group, self.parity = self.me // 2, self.me % 2
        self.partner = self.group * 2 + 1 - self.parity
        self.steps = sorted(range(1, self.groups), key=lambda d: min(d, self.groups - d))

    def slot(self, step, parity):
        return (self.group + step) % self.groups * 2 + parity

    def send(self, block, peer, number):
        ref = self.view(block)
        copy = remote(ref, ref, self.send_sems.at[number], self.recv_sems.at[block], self.axis, peer)
        copy.start()
        self.pending.append(copy)

    def wait(self, block):
        ref = self.view(block)
        remote(ref, ref, self.send_sems.at[0], self.recv_sems.at[block], self.axis, self.partner).wait_recv()

    def start(self):
        for number, step in enumerate(self.steps):
            self.send(self.me, self.slot(step, self.parity), number)
        self.send(self.me, self.partner, self.groups - 1)

    def arrivals(self):
        self.wait(self.partner)
        yield self.partner
        for number, step in enumerate(self.steps):
            block = self.slot(step, self.parity)
            self.wait(block)
            self.send(block, self.partner, self.groups + number)
            yield block
        for step in self.steps:
            block = self.slot(step, 1 - self.parity)
            self.wait(block)
            yield block


class Spread:
    def __init__(self, axis, size, view, send_sems, recv_sems, pending):
        self.axis, self.size, self.view, self.pending = axis, size, view, pending
        self.send_sems, self.recv_sems = send_sems, recv_sems
        self.me = lax.axis_index(axis)

    def start(self):
        ref = self.view(self.me)
        for step in range(1, self.size):
            copy = remote(
                ref, ref, self.send_sems.at[step - 1], self.recv_sems.at[self.me], self.axis, (self.me + step) % self.size
            )
            copy.start()
            self.pending.append(copy)

    def finish(self):
        for step in range(1, self.size):
            source = (self.me + step) % self.size
            ref = self.view(source)
            remote(ref, ref, self.send_sems.at[0], self.recv_sems.at[source], self.axis, source).wait_recv()


def rows_of(ref, size):
    return lambda i: ref.at[pl.ds(pl.multiple_of(i * size, size), size)]


def columns_of(ref, size):
    return lambda i: ref.at[:, pl.ds(pl.multiple_of(i * size, size), size)]


def kernel(
    n,
    t,
    inputs_hbm,
    values_hbm,
    decay_hbm,
    factor_hbm,
    mean_hbm,
    var_hbm,
    delta_ref,
    square_ref,
    grad_ref,
    decay_grad_ref,
    inputs,
    values,
    decay,
    mean,
    var,
    quarter,
    own_rows,
    total,
    projected,
    partial,
    out_y,
    in_y,
    out_z,
    in_z,
    ratio,
    decay_parts,
    square_tp,
    square_fs,
    load_sems,
    a_send,
    a_recv,
    o_send,
    o_recv,
    b_send,
    b_recv,
    y_send,
    y_recv,
    z_send,
    z_recv,
    d_send,
    d_recv,
    p_send,
    p_recv,
    q_send,
    q_recv,
    st_send,
    st_recv,
    sf_send,
    sf_recv,
):
    fs, tp = lax.axis_index("fs"), lax.axis_index("tp")
    group, parity = fs // 2, fs % 2
    partner = group * 2 + 1 - parity
    depth, width = factor_hbm.shape
    rank = width * t
    block_rows, owner_rows = rank // t, rank // n
    decay_width = inputs.shape[1] // t
    pending = []

    quarter_view = rows_of(quarter, depth)
    own_view = columns_of(own_rows, width)
    loads = [
        pltpu.make_async_copy(source, target, load_sems.at[i])
        for i, (source, target) in enumerate(
            (
                (factor_hbm, quarter_view(fs)),
                (factor_hbm, own_view(tp)),
                (decay_hbm, decay),
                (inputs_hbm, inputs),
                (values_hbm, values),
                (mean_hbm, mean),
                (var_hbm, var),
            )
        )
    ]
    for load in loads:
        load.start()

    barrier = pltpu.get_barrier_semaphore()
    for step in range(1, t):
        pl.semaphore_signal(barrier, inc=1, device_id={"tp": (tp + step) % t}, device_id_type=MESH)
    for step in range(1, n):
        pl.semaphore_signal(barrier, inc=1, device_id={"fs": (fs + step) % n}, device_id_type=MESH)
    pl.semaphore_wait(barrier, n + t - 2)

    a = Gather("fs", n, quarter_view, a_send, a_recv, pending)
    loads[0].wait()
    a.start()
    own = Gather("tp", t, own_view, o_send, o_recv, pending)
    loads[1].wait()
    own.start()

    loads[2].wait()
    loads[3].wait()
    decay_columns = pl.ds(pl.multiple_of(tp * decay_width, decay_width), decay_width)
    decay_parts[fs] = jnp.dot(decay[...], inputs[:, decay_columns], preferred_element_type=F32).astype(BF16)

    def project(block):
        at = pl.ds(pl.multiple_of(block * depth, depth), depth)
        return jnp.dot(inputs[:, at], quarter[at], preferred_element_type=F32)

    total[...] = project(fs)
    for block in a.arrivals():
        total[...] += project(block)

    projected_view = rows_of(projected, block_rows)
    projected_view(tp)[...] = total[...].T.astype(BF16)
    b = Gather("tp", t, projected_view, b_send, b_recv, pending)
    b.start()
    p = Spread("fs", n, lambda i: decay_parts.at[i], p_send, p_recv, pending)
    p.start()

    out_y_view, in_y_view = rows_of(out_y, owner_rows), rows_of(in_y, owner_rows)
    out_z_view, in_z_view = rows_of(out_z, owner_rows), rows_of(in_z, owner_rows)
    partial_view = rows_of(partial, owner_rows)
    per = n // t // 2

    def reduce_pair(block):
        rows_of(partial, block_rows)(block)[...] = jnp.dot(
            projected_view(block)[...], values[...], preferred_element_type=F32
        )
        for j in range(per):
            target = block * per + j
            out_y_view(target)[...] = partial_view(target * 2 + 1 - parity)[...].astype(BF16)
            copy = remote(
                out_y_view(target), in_y_view(target), y_send.at[target], y_recv.at[target], "fs", partner
            )
            copy.start()
            pending.append(copy)

    def reduce_groups(block):
        for j in range(per):
            target = block * per + j
            remote(
                out_y_view(target), in_y_view(target), y_send.at[target], y_recv.at[target], "fs", partner
            ).wait_recv()
            mine = partial_view(target * 2 + parity)
            mine[...] = mine[...] + in_y_view(target)[...].astype(F32)
            out_z_view(target)[...] = mine[...].astype(BF16)

            @pl.when(target != group)
            def _():
                remote(
                    out_z_view(target),
                    in_z_view(group),
                    z_send.at[target],
                    z_recv.at[group],
                    "fs",
                    target * 2 + parity,
                ).start()

    loads[4].wait()
    reduce_pair(tp)
    waiting = [tp]
    blocks = b.arrivals()
    for number in range(1, t):
        block = next(blocks)
        reduce_pair(block)
        waiting.append(block)
        if number % 2 == 1:
            for each in waiting:
                reduce_groups(each)
            waiting = []
    for _ in blocks:
        pass

    p.finish()
    decay_sum = decay_parts[0].astype(F32)
    for i in range(1, n):
        decay_sum += decay_parts[i].astype(F32)
    decay_grad_ref[:, decay_columns] = decay_sum
    q = Spread("tp", t, columns_of(decay_grad_ref, decay_width), q_send, q_recv, pending)
    q.start()
    for _ in own.arrivals():
        pass

    loads[5].wait()
    loads[6].wait()
    grad = partial_view(fs)[...]
    for step in range(1, n // 2):
        source = (group + step) % (n // 2)
        remote(
            out_z_view(source), in_z_view(source), z_send.at[source], z_recv.at[source], "fs", source * 2 + parity
        ).wait_recv()
        grad += in_z_view(source)[...].astype(F32)
    grad_ref[...] = grad
    mean_new, var_new = moments(mean[...], var[...], grad)
    adam_ratio = mean_new / (jnp.sqrt(var_new) + 1e-08)
    ratio_view = rows_of(ratio, owner_rows)
    ratio_view(fs)[...] = adam_ratio.astype(BF16)
    d = Gather("fs", n, ratio_view, d_send, d_recv, pending)
    d.start()

    squares = adam_ratio * adam_ratio
    squares = sum(squares[i : i + 8] for i in range(0, squares.shape[0], 8))
    square_tp[tp] = sum(squares[:, i : i + 128] for i in range(0, squares.shape[1], 128))
    st = Spread("tp", t, lambda i: square_tp.at[i], st_send, st_recv, pending)
    st.start()
    st.finish()
    square_fs[fs] = sum(square_tp[i] for i in range(t))
    sf = Spread("fs", n, lambda i: square_fs.at[i], sf_send, sf_recv, pending)
    sf.start()

    for _ in d.arrivals():
        pass
    delta_ref[...] = jnp.dot(own_rows[...], ratio[...], preferred_element_type=F32)
    sf.finish()
    square_ref[...] = sum(square_fs[i] for i in range(n))
    q.finish()
    for copy in pending:
        copy.wait_send()
    for step in range(1, n // 2):
        target = (group + step) % (n // 2)
        remote(
            out_z_view(target), in_z_view(target), z_send.at[target], z_recv.at[target], "fs", target * 2 + parity
        ).wait_send()


def fits(n, t, inputs, decay_cot, factor, mean):
    depth, width = factor.shape
    rank = width * t
    return (
        n % (2 * t) == 0
        and t % 2 == 0
        and mean.shape[0] % 16 == 0
        and mean.shape[1] % 128 == 0
        and mean.shape[0] * n == rank
        and depth % 128 == 0
        and width % 128 == 0
        and inputs.shape[0] % 128 == 0
        and inputs.shape[1] % (128 * t) == 0
        and decay_cot.shape[1] % 16 == 0
    )


def by_kernel(n, t, inputs, values_cot, decay_cot, factor, mean, var):
    tokens, model = inputs.shape
    depth, width = factor.shape
    columns = values_cot.shape[1]
    heads = decay_cot.shape[1]
    rank = width * t
    owner_rows = rank // n
    dma = lambda k: pltpu.SemaphoreType.DMA((k,))
    half = n // 2
    delta, square, grad, decay_grad = pl.pallas_call(
        functools.partial(kernel, n, t),
        out_shape=(
            jax.ShapeDtypeStruct((depth, columns), F32),
            jax.ShapeDtypeStruct((8, 128), F32),
            jax.ShapeDtypeStruct((owner_rows, columns), F32),
            jax.ShapeDtypeStruct((heads, model), F32),
        ),
        in_specs=[pl.BlockSpec(memory_space=pl.ANY)] * 6,
        out_specs=[pl.BlockSpec(memory_space=pltpu.VMEM)] * 4,
        scratch_shapes=[
            pltpu.VMEM((tokens, model), BF16),
            pltpu.VMEM((tokens, columns), BF16),
            pltpu.VMEM((heads, tokens), BF16),
            pltpu.VMEM((owner_rows, columns), F32),
            pltpu.VMEM((owner_rows, columns), F32),
            pltpu.VMEM((model, width), BF16),
            pltpu.VMEM((depth, rank), BF16),
            pltpu.VMEM((tokens, width), F32),
            pltpu.VMEM((rank, tokens), BF16),
            pltpu.VMEM((rank, columns), F32),
            pltpu.VMEM((rank // 2, columns), BF16),
            pltpu.VMEM((rank // 2, columns), BF16),
            pltpu.VMEM((rank // 2, columns), BF16),
            pltpu.VMEM((rank // 2, columns), BF16),
            pltpu.VMEM((rank, columns), BF16),
            pltpu.VMEM((n, heads, model // t), BF16),
            pltpu.VMEM((t, 8, 128), F32),
            pltpu.VMEM((n, 8, 128), F32),
            dma(7),
            dma(n),
            dma(n),
            dma(t),
            dma(t),
            dma(t),
            dma(t),
            dma(half),
            dma(half),
            dma(half),
            dma(half),
            dma(n),
            dma(n),
            dma(n),
            dma(n),
            dma(t),
            dma(t),
            dma(t),
            dma(t),
            dma(n),
            dma(n),
        ],
        compiler_params=pltpu.CompilerParams(collective_id=0, has_side_effects=True),
        name="lowrank",
    )(inputs, values_cot, decay_cot.T, factor, mean, var)
    return delta, jnp.sum(square), grad, decay_grad.T


def by_collectives(inputs, values_cot, decay_cot, factor, mean, var):
    own_rows = lax.all_gather(factor, "tp", axis=1, tiled=True)
    quarter = jnp.dot(
        inputs, lax.all_gather(factor, "fs", axis=0, tiled=True), preferred_element_type=F32
    ).astype(BF16)
    projected = lax.all_gather(quarter, "tp", axis=1, tiled=True)
    grad = lax.psum_scatter(
        lax.dot_general(projected, values_cot, (((0,), (0,)), ((), ())), preferred_element_type=F32),
        "fs",
        scatter_dimension=0,
        tiled=True,
    )
    mean_new, var_new = moments(mean, var, grad)
    adam_ratio = mean_new / (jnp.sqrt(var_new) + 1e-08)
    full_ratio = lax.all_gather(adam_ratio, "fs", axis=0, tiled=True)
    squares = lax.psum(jnp.sum(adam_ratio * adam_ratio), ("fs", "tp"))
    delta = jnp.dot(own_rows.astype(F32), full_ratio, precision=lax.Precision.HIGHEST)
    decay_part = lax.dot_general(inputs, decay_cot, (((0,), (0,)), ((), ())), preferred_element_type=F32)
    return delta, squares, grad, lax.psum(decay_part, "fs")


def local(
    n,
    t,
    inputs,
    values_cot,
    decay_cot,
    factor,
    value_weight,
    lowrank_mean,
    lowrank_var,
    decay_weight,
    decay_mean,
    decay_var,
):
    middle = inputs, values_cot, decay_cot, factor, lowrank_mean, lowrank_var
    if fits(n, t, inputs, decay_cot, factor, lowrank_mean):
        delta, squares, lowrank_grad, decay_grad = by_kernel(n, t, *middle)
    else:
        delta, squares, lowrank_grad, decay_grad = by_collectives(*middle)
    entries = lowrank_mean.size * n * t
    mean_new, var_new = moments(lowrank_mean, lowrank_var, lowrank_grad)
    root_mean = jnp.sqrt(squares / entries + 1e-06)
    value_step = -0.5 / root_mean * delta
    value_new = value_weight + value_step
    value_copy = value_new.astype(BF16)
    decay_mean_new, decay_var_new = moments(decay_mean, decay_var, decay_grad)
    decay_new = decay_weight - 0.5 * decay_mean_new / (jnp.sqrt(decay_var_new) + 1e-08)
    decay_copy = decay_new.astype(BF16)
    return (
        value_step,
        value_new,
        value_copy,
        mean_new,
        var_new,
        decay_new,
        decay_copy,
        decay_mean_new,
        decay_var_new,
    )


def solution(mesh):
    in_specs = (
        P("fs", None),
        P("fs", "tp"),
        P("fs", None),
        P("fs", "tp"),
        P("fs", "tp"),
        P("fs", "tp"),
        P("fs", "tp"),
        P(),
        P(),
        P(),
    )
    out_specs = (
        P("fs", "tp"),
        P("fs", "tp"),
        P("fs", "tp"),
        P("fs", "tp"),
        P("fs", "tp"),
        P(),
        P(),
        P(),
        P(),
    )
    body = functools.partial(local, mesh.shape["fs"], mesh.shape["tp"])
    return jax.shard_map(body, mesh=mesh, in_specs=in_specs, out_specs=out_specs, check_vma=False)
```

time: 249 us -> 54.3 us (0.22)
  waiting for transfers between devices: 127 us -> 0 us
  blocking collectives: 87.7 us -> 0 us
  Pallas kernels: 0 us -> 46.6 us
  between operations: 14.5 us -> 1.42 us
  local copies, waits for them, and re-layouts: 7.93 us -> 0.03 us
  matrix products: 7.14 us -> 0 us
    psum x1 -> x0, waiting for transfers between devices: 63.3 us -> none  [local(): decay_grad = lax.psum(decay_part, 'fs')]
    reduce_scatter x1 -> x0, waiting for transfers between devices: 63.2 us -> none  [local(): lax.psum_scatter(lax.dot_general(projected, values_cot, (((0,), (0,)), ((...]
    all_gather x3 -> x0, blocking collectives: 47.8 us -> none  [the longest x1 33.4 us: local(): lax.all_gather(factor, 'fs', axis=0, tiled=True)]
    pallas_call x0 -> x1, Pallas kernels: none -> 46.6 us  [by_kernel(): pl.pallas_call(functools.partial(kernel, n, t), out_shape=(jax.ShapeDtype...]
    psum x1 -> x0, blocking collectives: 39.9 us -> none  [local(): squares = lax.psum(jnp.sum(adam_ratio * adam_ratio), ('fs', 'tp'))]
    unnamed x16 -> x14, local copies, waits for them, and re-layouts: 7.93 us -> 0.03 us
    dot_general x4 -> x0, matrix products: 7.14 us -> none  [the longest x1 3.4 us: local(): jnp.dot(own_rows.astype(jnp.float32), full_ratio, precision=lax.Precision...]
  transfers between devices with their start and end apart: 3 -> 0, of which waited for: 2 -> 0; matrix products, arithmetic and copies ran while one was open for 3% -> 0% of each run, Pallas kernels for 0% -> 0%
where the time goes in v1:
time: 54.3 us; the launch traced here: 54.1 us
  Pallas kernels  46.6 us (86%)
  other arithmetic  6 us (11%)
  between operations  1.42 us (3%)
    pallas_call x1, Pallas kernels, by_kernel(): pl.pallas_call(functools.partial(kernel, n, t), out_shape=(jax.ShapeDtype...  46.6 us
    convert_element_type x1, other arithmetic, local(): value_copy = value_new.astype(BF16)  2.24 us
    convert_element_type x1, other arithmetic, local(): decay_copy = decay_new.astype(BF16)  1.7 us
    reduce_sum x1, other arithmetic, by_kernel(): return (delta, jnp.sum(square), grad, decay_grad.T)  1.32 us

profile of v1, /device:TPU:0, one launch (start us, length us, event | category | flops | bytes accessed | tf_op | source)
XLA Modules:
  0.0 54.1 jit_solution(2233716325066297208)
XLA Ops:
  0.6 0.0 copy-start
  0.7 0.0 copy-start.3
  0.7 0.0 copy-start.4
  0.7 0.0 copy-start.5
  0.7 0.0 copy-start.1
  0.7 0.0 copy-start.2
  0.7 46.6 %lowrank.1 = (f32[256,512]{1,0:T(8,128)}, f32[8,128]{1,0:T(8,128)}, f32[64,512]{1,0:T(8,128)}, f32[16,2048]{1,0:T(8,128)}) custom-call(bf16[768,2048]{1,0:T(8,128)(2,1)} %inputs_hbm.1, bf16[768,512]{1,0:T(8,128)(2,1)} %values_hbm.1, bf16[16,768]{1,0:T(8,128)(2,1)} %bitcast.8, bf16[256,128]{1,0:T(8,128)(2,1)} %factor_hbm.1, f32[64,512]{1,0:T(8,128)} %mean_hbm.1, ...), custom_call_target="tpu_custom_call" | custom-call | tf_op jit(solution)/shard_map/lowrank/pallas_call | solution.py:349
  47.3 0.0 copy-start.6
  47.3 1.3 %reduce_sum.9 = f32[]{:T(128)} reduce(f32[8,128]{1,0:T(8,128)} %get-tuple-element.13, f32[]{:T(128)} %constant.11.clone.1), dimensions={0,1}, to_apply=%region_0.0 | reduce | flops 1023 | bytes 4104 | tf_op jit(solution)/shard_map/reduce_sum | solution.py:403
  49.3 0.0 copy-done
  49.3 2.2 %fusion.6 = (bf16[256,512]{1,0:T(8,128)(2,1)}, f32[256,512]{1,0:T(8,128)}, f32[256,512]{1,0:T(8,128)}) fusion(f32[256,512]{1,0:T(8,128)S(1)} %copy-done, f32[256,512]{1,0:T(8,128)} %get-tuple-element.14, f32[]{:T(128)S(6)} %div.10), kind=kLoop, calls=%fused_computation.10 | loop fusion | flops 393216 | bytes 2359300 | tf_op jit(solution)/shard_map/convert_element_type | solution.py:451
  51.6 0.0 copy-done.3
  51.6 0.0 copy-done.4
  51.6 0.0 copy-done.5
  51.6 1.7 %fusion.3 = (bf16[2048,16]{0,1:T(8,128)(2,1)}, f32[2048,16]{0,1:T(8,128)}, f32[2048,16]{0,1:T(8,128)}, f32[2048,16]{0,1:T(8,128)}) fusion(f32[2048,16]{0,1:T(8,128)S(1)} %copy-done.3, f32[16,2048]{1,0:T(8,128)} %get-tuple-element.16, f32[2048,16]{0,1:T(8,128)S(1)} %copy-done.4, f32[2048,16]{0,1:T(8,128)S(1)} %copy-done.5), kind=kLoop, calls=%fused_computation.9 | loop fusion | flops 393216 | bytes 983040 | tf_op jit(solution)/shard_map/convert_element_type | solution.py:454
  53.3 0.0 copy-done.1
  53.3 0.0 copy-done.2
  53.3 0.0 copy-done.6
  53.3 0.7 %fusion = (f32[64,512]{1,0:T(8,128)}, f32[64,512]{1,0:T(8,128)}) fusion(f32[64,512]{1,0:T(8,128)S(1)} %copy-done.6, f32[64,512]{1,0:T(8,128)S(1)} %copy-done.2, f32[64,512]{1,0:T(8,128)S(1)} %copy-done.1), kind=kLoop, calls=%fused_computation.3 | loop fusion | flops 229376 | bytes 655360 | tf_op jit(solution)/shard_map/add | solution.py:16
Async XLA Ops:
  0.6 48.7 %copy-start = (f32[256,512]{1,0:T(8,128)S(1)}, f32[256,512]{1,0:T(8,128)}, u32[]{:S(2)}) copy-start(f32[256,512]{1,0:T(8,128)} %param.14) | copy-start | bytes 1572868
  0.7 50.9 %copy-start.3 = (f32[2048,16]{0,1:T(8,128)S(1)}, f32[2048,16]{0,1:T(8,128)}, u32[]{:S(2)}) copy-start(f32[2048,16]{0,1:T(8,128)} %param.17) | copy-start | bytes 393220
  0.7 50.9 %copy-start.4 = (f32[2048,16]{0,1:T(8,128)S(1)}, f32[2048,16]{0,1:T(8,128)}, u32[]{:S(2)}) copy-start(f32[2048,16]{0,1:T(8,128)} %param.18) | copy-start | bytes 393220
  0.7 50.9 %copy-start.5 = (f32[2048,16]{0,1:T(8,128)S(1)}, f32[2048,16]{0,1:T(8,128)}, u32[]{:S(2)}) copy-start(f32[2048,16]{0,1:T(8,128)} %param.19) | copy-start | bytes 393220
  0.7 52.6 %copy-start.1 = (f32[64,512]{1,0:T(8,128)S(1)}, f32[64,512]{1,0:T(8,128)}, u32[]{:S(2)}) copy-start(f32[64,512]{1,0:T(8,128)} %mean_hbm.1) | copy-start | bytes 393220
  0.7 52.6 %copy-start.2 = (f32[64,512]{1,0:T(8,128)S(1)}, f32[64,512]{1,0:T(8,128)}, u32[]{:S(2)}) copy-start(f32[64,512]{1,0:T(8,128)} %var_hbm.1) | copy-start | bytes 393220
  47.3 6.0 %copy-start.6 = (f32[64,512]{1,0:T(8,128)S(1)}, f32[64,512]{1,0:T(8,128)}, u32[]{:S(2)}) copy-start(f32[64,512]{1,0:T(8,128)} %get-tuple-element.15) | copy-start | bytes 393220

commit v2 on v1

--- a/solution.py
+++ b/solution.py
@@ -320,6 +320,64 @@
         ).wait_send()
 
 
+def finish(entries, *refs):
+    ins, outs, held, made, in_sems, out_sems = refs[:10], refs[10:19], refs[19:29], refs[29:38], refs[38], refs[39]
+    loads = [pltpu.make_async_copy(a, b, in_sems.at[i]) for i, (a, b) in enumerate(zip(ins, held))]
+    stores = [pltpu.make_async_copy(a, b, out_sems.at[i]) for i, (a, b) in enumerate(zip(made, outs))]
+    for load in loads:
+        load.start()
+    delta, square, weight, grad, mean, var, decay_grad, decay_mean, decay_var, decay_weight = held
+    step, new, copy, mean_new, var_new, decay_new, decay_copy, decay_mean_new, decay_var_new = made
+    for load in loads[:3]:
+        load.wait()
+    scale = -0.5 / jnp.sqrt(jnp.sum(square[...], keepdims=True) / entries + 1e-06)
+    step[...] = scale * delta[...]
+    stores[0].start()
+    new[...] = weight[...] + step[...]
+    stores[1].start()
+    copy[...] = new[...].astype(BF16)
+    stores[2].start()
+    for load in loads[3:]:
+        load.wait()
+    mean_new[...], var_new[...] = moments(mean[...], var[...], grad[...])
+    stores[3].start()
+    stores[4].start()
+    decay_mean_new[...], decay_var_new[...] = moments(decay_mean[...], decay_var[...], decay_grad[...])
+    stores[7].start()
+    stores[8].start()
+    decay_new[...] = decay_weight[...] - 0.5 * decay_mean_new[...] / (jnp.sqrt(decay_var_new[...]) + 1e-08)
+    stores[5].start()
+    decay_copy[...] = decay_new[...].astype(BF16)
+    stores[6].start()
+    for store in stores:
+        store.wait()
+
+
+def finish_by_kernel(entries, *args):
+    like = lambda x, dtype=F32: jax.ShapeDtypeStruct(x.shape, dtype)
+    weight, mean, decay_weight = args[2], args[4], args[9]
+    outs = (
+        like(weight),
+        like(weight),
+        like(weight, BF16),
+        like(mean),
+        like(mean),
+        like(decay_weight),
+        like(decay_weight, BF16),
+        like(decay_weight),
+        like(decay_weight),
+    )
+    return pl.pallas_call(
+        functools.partial(finish, entries),
+        out_shape=outs,
+        in_specs=[pl.BlockSpec(memory_space=pltpu.HBM)] * 10,
+        out_specs=[pl.BlockSpec(memory_space=pltpu.HBM)] * 9,
+        scratch_shapes=[pltpu.VMEM(x.shape, x.dtype) for x in args + outs]
+        + [pltpu.SemaphoreType.DMA((10,)), pltpu.SemaphoreType.DMA((9,))],
+        name="finish",
+    )(*args)
+
+
 def fits(n, t, inputs, decay_cot, factor, mean):
     depth, width = factor.shape
     rank = width * t
@@ -400,7 +458,7 @@
         compiler_params=pltpu.CompilerParams(collective_id=0, has_side_effects=True),
         name="lowrank",
     )(inputs, values_cot, decay_cot.T, factor, mean, var)
-    return delta, jnp.sum(square), grad, decay_grad.T
+    return delta, square, grad, decay_grad
 
 
 def by_collectives(inputs, values_cot, decay_cot, factor, mean, var):
@@ -439,11 +497,24 @@
     decay_var,
 ):
     middle = inputs, values_cot, decay_cot, factor, lowrank_mean, lowrank_var
+    entries = lowrank_mean.size * n * t
     if fits(n, t, inputs, decay_cot, factor, lowrank_mean):
-        delta, squares, lowrank_grad, decay_grad = by_kernel(n, t, *middle)
-    else:
-        delta, squares, lowrank_grad, decay_grad = by_collectives(*middle)
-    entries = lowrank_mean.size * n * t
+        delta, square, lowrank_grad, decay_grad = by_kernel(n, t, *middle)
+        outs = finish_by_kernel(
+            entries,
+            delta,
+            square,
+            value_weight,
+            lowrank_grad,
+            lowrank_mean,
+            lowrank_var,
+            decay_grad,
+            decay_mean.T,
+            decay_var.T,
+            decay_weight.T,
+        )
+        return outs[:5] + tuple(x.T for x in outs[5:])
+    delta, squares, lowrank_grad, decay_grad = by_collectives(*middle)
     mean_new, var_new = moments(lowrank_mean, lowrank_var, lowrank_grad)
     root_mean = jnp.sqrt(squares / entries + 1e-06)
     value_step = -0.5 / root_mean * delta

time: 54.3 us -> 50.2 us (0.924)
  other arithmetic: 6 us -> 0 us
  Pallas kernels: 46.6 us -> 49.4 us
  between operations: 1.42 us -> 0.65 us
    convert_element_type x2 -> x0, other arithmetic: 3.94 us -> none  [the longest x1 2.24 us: local(): value_copy = value_new.astype(BF16)]
    pallas_call x0 -> x1, Pallas kernels: none -> 2.82 us  [finish_by_kernel(): pl.pallas_call(functools.partial(finish, entries), out_shape=outs, in_spe...]
    reduce_sum x1 -> x0, other arithmetic: 1.32 us -> none  [by_kernel(): return (delta, jnp.sum(square), grad, decay_grad.T)]
    add x1 -> x0, other arithmetic: 0.74 us -> none  [moments(): return (0.9 * mean + 0.1 * grad, 0.95 * var + 0.05 * grad * grad)]
where the time goes in v2:
time: 50.2 us; the launch traced here: 50.1 us
  Pallas kernels  49.4 us (98%)
  between operations  0.65 us (1%)
    pallas_call x1, Pallas kernels, by_kernel(): pl.pallas_call(functools.partial(kernel, n, t), out_shape=(jax.ShapeDtype...  46.6 us
    pallas_call x1, Pallas kernels, finish_by_kernel(): pl.pallas_call(functools.partial(finish, entries), out_shape=outs, in_spe...  2.82 us

profile of v2, /device:TPU:0, one launch (start us, length us, event | category | flops | bytes accessed | tf_op | source)
XLA Modules:
  0.0 50.1 jit_solution(1870303792210811578)
XLA Ops:
  0.6 46.6 %lowrank.1 = (f32[256,512]{1,0:T(8,128)}, f32[8,128]{1,0:T(8,128)}, f32[64,512]{1,0:T(8,128)}, f32[16,2048]{1,0:T(8,128)}) custom-call(bf16[768,2048]{1,0:T(8,128)(2,1)} %inputs_hbm.1, bf16[768,512]{1,0:T(8,128)(2,1)} %values_hbm.1, bf16[16,768]{1,0:T(8,128)(2,1)} %bitcast.11, bf16[256,128]{1,0:T(8,128)(2,1)} %factor_hbm.1, f32[64,512]{1,0:T(8,128)} %refs_4_.1, ...), custom_call_target="tpu_custom_call" | custom-call | tf_op jit(solution)/shard_map/lowrank/pallas_call | solution.py:407
  47.2 2.8 %finish.1 = (f32[256,512]{1,0:T(8,128)}, f32[256,512]{1,0:T(8,128)}, bf16[256,512]{1,0:T(8,128)(2,1)}, f32[64,512]{1,0:T(8,128)}, f32[64,512]{1,0:T(8,128)}, /*i...) custom-call(f32[256,512]{1,0:T(8,128)} %get-tuple-element.22.refs_0_, ...), custom_call_target="tpu_custom_call" | custom-call | tf_op jit(solution)/shard_map/finish/pallas_call | solution.py:370

commit v3 on v2

--- a/solution.py
+++ b/solution.py
@@ -255,16 +255,14 @@
 
     loads[4].wait()
     reduce_pair(tp)
-    waiting = [tp]
+    before = tp
     blocks = b.arrivals()
     for number in range(1, t):
         block = next(blocks)
         reduce_pair(block)
-        waiting.append(block)
-        if number % 2 == 1:
-            for each in waiting:
-                reduce_groups(each)
-            waiting = []
+        reduce_groups(before)
+        before = block
+    reduce_groups(before)
     for _ in blocks:
         pass
 

time: 50.2 us -> 49.6 us (0.988)
  Pallas kernels: 49.4 us -> 48.8 us
    pallas_call x1, Pallas kernels: 46.6 us -> 45.9 us  [by_kernel(): pl.pallas_call(functools.partial(kernel, n, t), out_shape=(jax.ShapeDtype...]
where the time goes in v3:
time: 49.6 us; the launch traced here: 49.4 us
  Pallas kernels  48.8 us (98%)
  between operations  0.65 us (1%)
    pallas_call x1, Pallas kernels, by_kernel(): pl.pallas_call(functools.partial(kernel, n, t), out_shape=(jax.ShapeDtype...  45.9 us
    pallas_call x1, Pallas kernels, finish_by_kernel(): pl.pallas_call(functools.partial(finish, entries), out_shape=outs, in_spe...  2.82 us

profile of v3, /device:TPU:0, one launch (start us, length us, event | category | flops | bytes accessed | tf_op | source)
XLA Modules:
  0.0 49.4 jit_solution(16501199838231240631)
XLA Ops:
  0.6 45.9 %lowrank.1 = (f32[256,512]{1,0:T(8,128)}, f32[8,128]{1,0:T(8,128)}, f32[64,512]{1,0:T(8,128)}, f32[16,2048]{1,0:T(8,128)}) custom-call(bf16[768,2048]{1,0:T(8,128)(2,1)} %inputs_hbm.1, bf16[768,512]{1,0:T(8,128)(2,1)} %values_hbm.1, bf16[16,768]{1,0:T(8,128)(2,1)} %bitcast.11, bf16[256,128]{1,0:T(8,128)(2,1)} %factor_hbm.1, f32[64,512]{1,0:T(8,128)} %refs_4_.1, ...), custom_call_target="tpu_custom_call" | custom-call | tf_op jit(solution)/shard_map/lowrank/pallas_call | solution.py:405
  46.6 2.8 %finish.1 = (f32[256,512]{1,0:T(8,128)}, f32[256,512]{1,0:T(8,128)}, bf16[256,512]{1,0:T(8,128)(2,1)}, f32[64,512]{1,0:T(8,128)}, f32[64,512]{1,0:T(8,128)}, /*i...) custom-call(f32[256,512]{1,0:T(8,128)} %get-tuple-element.22.refs_0_, ...), custom_call_target="tpu_custom_call" | custom-call | tf_op jit(solution)/shard_map/finish/pallas_call | solution.py:368
